TPU v7x, 32 devices: a whole 2x2x4 slice. The times are simulated.
32 devices in a mesh: ep: 16 (over z, y, x), tp: 2 (over core).
Axes of the slice: x: 2, y: 2, z: 4, core: 2. Of those that a mesh axis runs over, the one named last changes fastest.
Arguments:
- tokens: bfloat16 [384, 2048], P('ep'), may hold values from -6 to 6
- attn_gain: float32 [2048], replicated, may hold values from 0.1 to 1.9
- w_query: bfloat16 [2048, 1024], P(None, 'tp'), may hold values from -0.125 to 0.125
- w_key: bfloat16 [2048, 1024], P(None, 'tp'), may hold values from -0.125 to 0.125
- w_value: bfloat16 [2048, 1024], P(None, 'tp'), may hold values from -0.125 to 0.125
- w_zgate: bfloat16 [2048, 1024], P(None, 'tp'), may hold values from -0.125 to 0.125
- w_decay: bfloat16 [2048, 8], P(None, 'tp'), may hold values from -0.125 to 0.125
- w_beta: bfloat16 [2048, 8], P(None, 'tp'), may hold values from -0.125 to 0.125
- decay_rate: float32 [8], P('tp'), may hold values from 0.05 to 2
- decay_bias: float32 [8], P('tp'), may hold values from -3 to 3
- state: float32 [384, 8, 128, 128], P('ep', 'tp'), may hold values from -2 to 2
- out_gain: float32 [128], replicated, may hold values from 0.1 to 1.9
- w_out: bfloat16 [1024, 2048], P('tp'), may hold values from -0.1875 to 0.1875
- ffn_gain: float32 [2048], replicated, may hold values from 0.1 to 1.9
- expert_gate: bfloat16 [16, 2048, 512], P('ep', None, 'tp'), may hold values from -0.125 to 0.125
- expert_up: bfloat16 [16, 2048, 512], P('ep', None, 'tp'), may hold values from -0.125 to 0.125
- expert_down: bfloat16 [16, 512, 2048], P('ep', 'tp'), may hold values from -0.25 to 0.25
- routes: int32 [384, 2], P('ep'), may hold values from 0 to 15, all different within a row; in each aligned block of 24 rows (0 to 23, 24 to 47, ...) at most 6 rows name the same one
- route_weight: float32 [384, 2], P('ep'), may hold values from 0.2 to 1
Outputs:
- layer_out: bfloat16 [384, 2048], P('ep', 'tp')
- new_state: float32 [384, 8, 128, 128], P('ep', 'tp')
Inputs may be any that keep to these rules, and one draw needn't show every extreme that they name: `routes`: the 2 entries of a row differ. Among the rows of one index of ep (aligned blocks of 24 rows) no expert is named more than 6 times, a bound that some block reaches.
All inputs are finite; a program needn't handle non-finite values.
Results may differ from a plain program's by a relative error of at most 0.014.
Values may be sent and summed in bfloat16 or wider, within the bound.
A program may use at most 128 MiB of HBM per device.

v0:
```python
import jax
import jax.numpy as jnp
from jax import lax
from jax.sharding import PartitionSpec as P

EPS = 1e-06


def rms_scale(rows, gain):
    return rows * lax.rsqrt(jnp.mean(rows * rows, axis=-1, keepdims=True) + EPS) * gain


def unit_rows(rows):
    return rows * lax.rsqrt(jnp.sum(rows * rows, axis=-1, keepdims=True) + EPS)


def per_device(
    tokens,
    attn_gain,
    w_query,
    w_key,
    w_value,
    w_zgate,
    w_decay,
    w_beta,
    decay_rate,
    decay_bias,
    state,
    out_gain,
    w_out,
    ffn_gain,
    expert_gate,
    expert_up,
    expert_down,
    routes,
    route_weight,
):
    seqs, width = tokens.shape
    heads = state.shape[1]
    head_dim = state.shape[2]
    top = routes.shape[1]
    resid_in = tokens.astype(jnp.float32)
    normed = rms_scale(resid_in, attn_gain).astype(jnp.bfloat16)

    def project(weight):
        return jnp.dot(normed, weight, preferred_element_type=jnp.float32).astype(jnp.bfloat16)

    def heads_of(raw):
        return raw.reshape(seqs, heads, head_dim).astype(jnp.float32)

    query = unit_rows(jax.nn.silu(heads_of(project(w_query)))) * head_dim ** (-0.5)
    key = unit_rows(jax.nn.silu(heads_of(project(w_key))))
    value = jax.nn.silu(heads_of(project(w_value)))
    zmul = jax.nn.silu(heads_of(project(w_zgate)))
    fade = jnp.exp(-decay_rate * jax.nn.softplus(project(w_decay).astype(jnp.float32) + decay_bias))
    beta = jax.nn.sigmoid(project(w_beta).astype(jnp.float32))
    predicted = jnp.einsum("shkv,shk->shv", state, key, precision=lax.Precision.HIGHEST)
    written = beta[..., None] * (value - fade[..., None] * predicted)
    new_state = fade[..., None, None] * state + key[..., :, None] * written[..., None, :]
    read = jnp.einsum("shkv,shk->shv", new_state, query, precision=lax.Precision.HIGHEST)
    heads_out = (
        (rms_scale(read, out_gain) * zmul).astype(jnp.bfloat16).reshape(seqs, heads * head_dim)
    )
    partial_value = jnp.dot(heads_out, w_out, preferred_element_type=jnp.float32)
    mixed = lax.psum(partial_value.astype(jnp.bfloat16), "tp").astype(jnp.float32)
    resid = resid_in + mixed
    moe_in = rms_scale(resid, ffn_gain).astype(jnp.bfloat16)
    experts = lax.axis_size("ep")
    cap = max(2, 2 * seqs * top // experts)
    flat_routes = routes.reshape(-1)
    onehot = (flat_routes[:, None] == jnp.arange(experts, dtype=jnp.int32)[None, :]).astype(
        jnp.int32
    )
    before = jnp.cumsum(onehot, axis=0) - onehot
    slot = jnp.sum(before * onehot, axis=1)
    place = flat_routes * cap + slot
    pick = (place[:, None] == jnp.arange(experts * cap, dtype=jnp.int32)[None, :]).astype(
        jnp.bfloat16
    )
    columns = width // lax.axis_size("tp")
    own_part = lax.dynamic_slice_in_dim(moe_in, lax.axis_index("tp") * columns, columns, 1)
    spread = jnp.repeat(own_part, top, axis=0)
    outgoing = jnp.dot(pick.T, spread, preferred_element_type=jnp.float32).astype(jnp.bfloat16)
    outgoing = outgoing.reshape(experts, 1, cap, columns)
    arrived = lax.all_gather(
        lax.all_to_all(outgoing, "ep", split_axis=0, concat_axis=1, tiled=True),
        "tp",
        axis=3,
        tiled=True,
    )
    flat_rows = arrived.reshape(-1, arrived.shape[-1])
    gate = jnp.dot(flat_rows, expert_gate[0], preferred_element_type=jnp.float32)
    up = jnp.dot(flat_rows, expert_up[0], preferred_element_type=jnp.float32)
    hidden = (jax.nn.silu(gate) * up).astype(jnp.bfloat16)
    term = jnp.dot(hidden, expert_down[0], preferred_element_type=jnp.float32)
    terms = term.reshape(arrived.shape[:-1] + (term.shape[-1],))
    summed = lax.psum_scatter(terms.astype(jnp.bfloat16), "tp", scatter_dimension=3, tiled=True)
    returned = lax.all_to_all(summed, "ep", split_axis=1, concat_axis=0, tiled=True)
    returned = returned.reshape(experts * cap, columns)
    per_route = jnp.dot(pick, returned, preferred_element_type=jnp.float32).reshape(
        seqs, top, columns
    )
    combined = jnp.sum(per_route * route_weight[..., None], axis=1)
    own_resid = lax.dynamic_slice_in_dim(resid, lax.axis_index("tp") * columns, columns, 1)
    layer_out = (own_resid + combined).astype(jnp.bfloat16)
    return (layer_out, new_state)


def solution(mesh):
    in_specs = (
        P("ep", None),
        P(),
        P(None, "tp"),
        P(None, "tp"),
        P(None, "tp"),
        P(None, "tp"),
        P(None, "tp"),
        P(None, "tp"),
        P("tp"),
        P("tp"),
        P("ep", "tp", None, None),
        P(),
        P("tp", None),
        P(),
        P("ep", None, "tp"),
        P("ep", None, "tp"),
        P("ep", "tp", None),
        P("ep", None),
        P("ep", None),
    )
    out_specs = (P("ep", "tp"), P("ep", "tp", None, None))
    return jax.shard_map(
        per_device, mesh=mesh, in_specs=in_specs, out_specs=out_specs, check_vma=False
    )
```

profile of v0, /device:TPU:0, one launch (start us, length us, event | category | flops | bytes accessed | tf_op | source)
XLA Modules:
  0.0 115.3 jit_solution(10898759450930380615)
XLA Ops:
  7.3 1.2 %fusion.18 = f32[24]{0:T(128)S(1)} fusion(bf16[24,2048]{1,0:T(8,128)(2,1)} %param.19), kind=kLoop, calls=%fused_computation.33 | loop fusion | flops 147432 | bytes 98400 | tf_op jit(solution)/shard_map/reduce_sum | solution.py:10
  8.5 2.1 %fusion.6 = f32[24,512]{1,0:T(8,128)S(1)} fusion(bf16[2048,512]{1,0:T(8,128)(2,1)} %param.22, bf16[24,2048]{1,0:T(8,128)(2,1)} %param.19, f32[2048]{0:T(1024)} %param.20, f32[24]{0:T(128)S(1)} %add_rsqrt_fusion.4), kind=kOutput, calls=%fused_computation.16 | convolution fusion | flops 50552832 | bytes 2252896 | tf_op jit(solution)/shard_map/dot_general | solution.py:46
  10.6 0.1 multiply_reduce_fusion.3
  10.7 0.1 broadcast_multiply_fusion
  10.9 0.2 fusion.34
  11.1 0.1 copy.48
  11.2 2.0 %fusion.5 = f32[24,512]{1,0:T(8,128)S(1)} fusion(bf16[2048,512]{1,0:T(8,128)(2,1)} %param.23, bf16[24,2048]{1,0:T(8,128)(2,1)S(1)} %copy-done.2, f32[2048]{0:T(1024)S(1)} %copy-done.5, f32[24]{0:T(128)S(1)} %add_rsqrt_fusion.4), kind=kOutput, calls=%fused_computation.14 | convolution fusion | flops 50552832 | bytes 2252896 | tf_op jit(solution)/shard_map/dot_general | solution.py:46
  13.3 0.2 fusion.13
  13.5 0.1 copy.49
  13.6 8.1 %fusion.41 = f32[24,4,1,128]{3,2,1,0:T(1,128)S(1)} fusion(f32[24,4,128,1]{2,3,1,0:T(1,128)S(1)} %bitcast.48, f32[24,4,128,128]{3,2,1,0:T(8,128)} %param.29), kind=kOutput, calls=%fused_computation.73 | convolution fusion | flops 18874368 | bytes 6389760 | tf_op jit(solution)/shard_map/shkv,shk->shv/dot_general | solution.py:57
  21.7 0.1 fusion.24
  21.8 3.9 %multiply_add_fusion = f32[24,4,128,128]{3,2,1,0:T(8,128)} fusion(f32[24,4,128,128]{3,2,1,0:T(8,128)S(1)} %copy-done.1, f32[24,4,128]{2,1,0:T(4,128)S(1)} %fusion.24, f32[24,4,128]{2,1,0:T(4,128)S(1)} %broadcast_multiply_fusion, f32[24,4]{1,0:T(8,128)S(1)} %copy.48), kind=kLoop, calls=%fused_computation | loop fusion | flops 4718592 | bytes 12681600 | tf_op jit(solution)/shard_map/add | solution.py:59
  25.7 0.4 fusion.4
  26.2 0.1 multiply_reduce_fusion.2
  26.3 0.1 multiply_multiply_fusion
  26.4 7.5 %fusion.42 = f32[24,4,1,128]{3,2,1,0:T(1,128)S(1)} fusion(f32[24,4,128,128]{3,2,1,0:T(8,128)} %multiply_add_fusion, f32[24,4,128,1]{2,3,1,0:T(1,128)S(1)} %bitcast.51), kind=kOutput, calls=%fused_computation.74 | convolution fusion | flops 18874368 | bytes 6389760 | tf_op jit(solution)/shard_map/shkv,shk->shv/dot_general | solution.py:60
  33.9 0.1 multiply_reduce_fusion.1
  34.1 0.4 fusion.3
  34.6 0.0 copy-done.9
  34.6 0.1 fusion.25
  34.7 1.0 convolution_convert_fusion.1
  35.8 0.0 reduce-scatter.2.cloned.1.call-start
  35.8 0.1 copy.51
  35.9 0.1 eq.50
  36.0 0.1 fusion.28
  36.1 0.1 reduce_window_sum.11
  36.2 0.2 select_reduce_fusion
  36.4 20.1 %all-reduce.2.cloned.1.call-done = bf16[24,2048]{1,0:T(8,128)(2,1)} async-done(((bf16[24,2048]{1,0:T(8,128)(2,1)}), bf16[24,2048]{1,0:T(8,128)(2,1)}) %all-reduce.2.cloned.1.call-update) | async-done | bytes 98320 | tf_op jit(solution)/shard_map/psum | solution.py:65
  56.5 1.0 multiply_reduce_fusion
  57.5 0.1 multiply_convert_fusion
  57.6 0.1 broadcast_in_dim.2
  57.7 0.3 convolution_convert_fusion.2
  58.0 0.1 reshape.136
  58.1 16.9 %all_to_all.21 = bf16[16,1,6,1024]{3,2,1,0:T(8,128)(2,1)S(1)} all-to-all(bf16[16,1,6,1024]{3,2,1,0:T(8,128)(2,1)S(1)} %bitcast.47), channel_id=1, replica_groups=mesh['ep'=16,'tp'=2] {'ep'}, dimensions={0} | all-to-all | bytes 393216 | tf_op jit(solution)/shard_map/all_to_all | solution.py:86
  75.0 2.2 %all-gather = bf16[16,1,6,2048]{3,2,1,0:T(8,128)(2,1)S(1)} all-gather(bf16[16,1,6,1024]{3,2,1,0:T(8,128)(2,1)S(1)} %all_to_all.21), channel_id=2, replica_groups=mesh['ep'=16,'tp'=2] {'tp'}, dimensions={3}, use_global_device_ids=true | all-gather | bytes 589824 | tf_op jit(solution)/shard_map/all_gather | solution.py:85
  77.2 0.1 reshape.137
  77.3 1.5 %fusion.16 = f32[96,256]{1,0:T(8,128)S(1)} fusion(bf16[96,2048]{1,0:T(8,128)(2,1)S(1)} %reshape.137, bf16[1,2048,256]{2,1,0:T(8,128)(2,1)} %param.33), kind=kOutput, calls=%fused_computation.28 | convolution fusion | flops 100663296 | bytes 1540096 | tf_op jit(solution)/shard_map/dot_general | solution.py:92
  78.9 1.5 %fusion.2 = bf16[96,256]{1,0:T(8,128)(2,1)S(1)} fusion(bf16[96,2048]{1,0:T(8,128)(2,1)S(1)} %reshape.137, bf16[1,2048,256]{2,1,0:T(8,128)(2,1)} %param.34, f32[96,256]{1,0:T(8,128)S(1)} %fusion.16), kind=kOutput, calls=%fused_computation.8 | convolution fusion | flops 100810752 | bytes 1589248 | tf_op jit(solution)/shard_map/dot_general | solution.py:93
  80.5 2.3 %fusion = bf16[1,16,6,2048]{3,1,2,0:T(8,128)(2,1)} fusion(bf16[1,256,2048]{2,1,0:T(8,128)(2,1)} %param.35, bf16[16,6,256]{2,1,0:T(8,128)(2,1)S(1)} %dot_general.56), kind=kOutput, calls=%fused_computation.2 | convolution fusion | flops 100859904 | bytes 1490944 | tf_op jit(solution)/shard_map/dot_general | solution.py:95
  82.8 5.9 %reduce-scatter.2.cloned.1.call-done = bf16[1,16,6,1024]{3,1,2,0:T(8,128)(2,1)} async-done(((bf16[1,16,6,2048]{3,1,2,0:T(8,128)(2,1)}), bf16[1,16,6,1024]{3,1,2,0:T(8,128)(2,1)}) %reduce-scatter.2.cloned.1.call-update) | async-done | bytes 196624 | tf_op jit(solution)/shard_map/reduce_scatter | solution.py:97
  88.6 1.7 %copy.55 = bf16[1,16,6,1024]{3,2,0,1:T(8,128)(2,1)} copy(bf16[1,16,6,1024]{3,1,2,0:T(8,128)(2,1)} %reduce-scatter.2.cloned.1.call-done) | data formatting | bytes 393216 | tf_op jit(solution)/shard_map/reduce_scatter | solution.py:97
  90.4 6.7 %all-to-all-start.1 = ((bf16[1,16,6,1024]{3,2,0,1:T(8,128)(2,1)}), bf16[1,16,6,1024]{3,2,0,1:T(8,128)(2,1)S(1)}, u32[]{:S(2)}, u32[]{:S(2)}) async-start(bf16[1,16,6,1024]{3,2,0,1:T(8,128)(2,1)} %copy.55), calls=%async_computation.2 | async-start | bytes 524288 | tf_op jit(solution)/shard_map/all_to_all | solution.py:98
  97.1 0.1 reduce_sum.70
  97.2 0.1 copy.52
  97.3 10.2 %all-to-all-done.1 = bf16[1,16,6,1024]{3,2,0,1:T(8,128)(2,1)S(1)} async-done(((bf16[1,16,6,1024]{3,2,0,1:T(8,128)(2,1)}), bf16[1,16,6,1024]{3,2,0,1:T(8,128)(2,1)S(1)}, u32[]{:S(2)}, u32[]{:S(2)}) %all-to-all-start.1) | async-done | bytes 196640 | tf_op jit(solution)/shard_map/all_to_all | solution.py:98
  107.5 0.1 reshape.150
  107.6 0.2 fusion.1
  107.8 0.6 add_convert_fusion
  (45 shorter events, 0.4 us)
Async XLA Ops:
  7.2 27.5 %copy-start = (bf16[512,2048]{1,0:T(8,128)(2,1)S(1)}, bf16[512,2048]{1,0:T(8,128)(2,1)}, u32[]{:S(2)}) copy-start(bf16[512,2048]{1,0:T(8,128)(2,1)} %param.31) | copy-start | bytes 6291460
  7.2 3.7 %copy-start.2 = (bf16[24,2048]{1,0:T(8,128)(2,1)S(1)}, bf16[24,2048]{1,0:T(8,128)(2,1)}, u32[]{:S(2)}) copy-start(bf16[24,2048]{1,0:T(8,128)(2,1)} %param.19) | copy-start | bytes 294916
  7.2 3.7 %copy-start.5 = (f32[2048]{0:T(1024)S(1)}, f32[2048]{0:T(1024)}, u32[]{:S(2)}) copy-start(f32[2048]{0:T(1024)} %param.20) | copy-start | bytes 24580
  7.2 3.6 %copy-start.12 = (f32[4]{0:T(128)S(1)}, f32[4]{0:T(128)}, u32[]{:S(2)}) copy-start(f32[4]{0:T(128)} %param.27) | copy-start | bytes 52
  7.2 3.7 %copy-start.10 = (bf16[2048,4]{0,1:T(4,128)(2,1)S(1)}, bf16[2048,4]{0,1:T(4,128)(2,1)}, u32[]{:S(2)}) copy-start(bf16[2048,4]{0,1:T(4,128)(2,1)} %param.25) | copy-start | bytes 49156
  7.2 3.7 %copy-start.13 = (f32[4]{0:T(128)S(1)}, f32[4]{0:T(128)}, u32[]{:S(2)}) copy-start(f32[4]{0:T(128)} %param.28) | copy-start | bytes 52
  7.2 49.2 %all-reduce.2.cloned.1.call-start = ((), (), s32[]{:S(2)}) async-start(), calls=%async_computation.3 | async-start | bytes 196608 | tf_op jit(solution)/shard_map/psum | solution.py:65
  8.4 4.8 %copy-start.11 = (bf16[2048,4]{0,1:T(4,128)(2,1)S(1)}, bf16[2048,4]{0,1:T(4,128)(2,1)}, u32[]{:S(2)}) copy-start(bf16[2048,4]{0,1:T(4,128)(2,1)} %param.26) | copy-start | bytes 49156
  13.6 8.2 %copy-start.1 = (f32[24,4,128,128]{3,2,1,0:T(8,128)S(1)}, f32[24,4,128,128]{3,2,1,0:T(8,128)}, u32[]{:S(2)}) copy-start(f32[24,4,128,128]{3,2,1,0:T(8,128)} %param.29) | copy-start | bytes 18874372
  21.8 3.9 %copy-start.3 = (bf16[2048,512]{1,0:T(8,128)(2,1)S(1)}, bf16[2048,512]{1,0:T(8,128)(2,1)}, u32[]{:S(2)}) copy-start(bf16[2048,512]{1,0:T(8,128)(2,1)} %param.21) | copy-start | bytes 6291460
  26.4 7.7 %copy-start.4 = (bf16[2048,512]{1,0:T(8,128)(2,1)S(1)}, bf16[2048,512]{1,0:T(8,128)(2,1)}, u32[]{:S(2)}) copy-start(bf16[2048,512]{1,0:T(8,128)(2,1)} %param.24) | copy-start | bytes 6291460
  33.9 0.7 copy-start.9
  34.1 1.7 %copy-start.6 = (s32[24,2]{0,1:T(2,128)S(1)}, s32[24,2]{0,1:T(2,128)}, u32[]{:S(2)}) copy-start(s32[24,2]{0,1:T(2,128)} %param.36) | copy-start | bytes 580
  34.1 2.3 %copy-start.7 = (f32[2048]{0:T(1024)S(1)}, f32[2048]{0:T(1024)}, u32[]{:S(2)}) copy-start(f32[2048]{0:T(1024)} %param.32) | copy-start | bytes 24580
  35.8 52.9 %reduce-scatter.2.cloned.1.call-start = ((), (), s32[]{:S(2)}) async-start(), calls=%async_computation.4 | async-start | bytes 589824 | tf_op jit(solution)/shard_map/reduce_scatter | solution.py:97
  80.4 27.2 %copy-start.8 = (f32[24,2]{0,1:T(2,128)S(1)}, f32[24,2]{0,1:T(2,128)}, u32[]{:S(2)}) copy-start(f32[24,2]{0,1:T(2,128)} %param.37) | copy-start | bytes 580
  90.4 17.1 %all-to-all-start.1 = ((bf16[1,16,6,1024]{3,2,0,1:T(8,128)(2,1)}), bf16[1,16,6,1024]{3,2,0,1:T(8,128)(2,1)S(1)}, u32[]{:S(2)}, u32[]{:S(2)}) async-start(bf16[1,16,6,1024]{3,2,0,1:T(8,128)(2,1)} %copy.55), calls=%async_computation.2 | async-start | bytes 524288 | tf_op jit(solution)/shard_map/all_to_all | solution.py:98
Sparse Core Ops, SparseCore 0:
  35.9 20.5 all-reduce.1
  82.9 5.7 reduce-scatter.1
where the time goes:
time: 116 us; the launch traced here: 115 us
  waiting for transfers between devices  36.2 us (31%)
  matrix products  28 us (24%)
  blocking collectives  19.1 us (16%)
  between operations  14.4 us (12%)
  other arithmetic  7.91 us (7%)
  starting transfers between devices  6.81 us (6%)
  local copies, waits for them, and re-layouts  2.86 us (2%)
    psum x1, waiting for transfers between devices, per_device(): lax.psum(partial_value.astype(jnp.bfloat16), 'tp').astype(jnp.float32)  20.1 us
    all_to_all x1, blocking collectives, per_device(): lax.all_to_all(outgoing, 'ep', split_axis=0, concat_axis=1, tiled=True)  16.9 us
    all_to_all x1, waiting for transfers between devices, per_device(): lax.all_to_all(summed, 'ep', split_axis=1, concat_axis=0, tiled=True)  10.2 us
    dot_general x1, matrix products, per_device(): jnp.einsum('shkv,shk->shv', state, key, precision=lax.Precision.HIGHEST)  8.09 us
    dot_general x1, matrix products, per_device(): jnp.einsum('shkv,shk->shv', new_state, query, precision=lax.Precision.HIG...  7.54 us
    all_to_all x1, starting transfers between devices, per_device(): lax.all_to_all(summed, 'ep', split_axis=1, concat_axis=0, tiled=True)  6.73 us
    reduce_scatter x1, waiting for transfers between devices, per_device(): lax.psum_scatter(terms.astype(jnp.bfloat16), 'tp', scatter_dimension=3, t...  5.89 us
    dot_general x6, matrix products, project(): jnp.dot(normed, weight, preferred_element_type=jnp.float32)  5.45 us
  transfers between devices with their start and end apart: 3, of which 3 were waited for; matrix products, arithmetic and copies ran while one was open for 1% of the time, Pallas kernels for 0%

commit v1 on v0

--- a/solution.py
+++ b/solution.py
@@ -62,7 +62,9 @@
         (rms_scale(read, out_gain) * zmul).astype(jnp.bfloat16).reshape(seqs, heads * head_dim)
     )
     partial_value = jnp.dot(heads_out, w_out, preferred_element_type=jnp.float32)
-    mixed = lax.psum(partial_value.astype(jnp.bfloat16), "tp").astype(jnp.float32)
+    mixed = jnp.sum(lax.all_gather(partial_value.astype(jnp.bfloat16), "tp"), axis=0).astype(
+        jnp.float32
+    )
     resid = resid_in + mixed
     moe_in = rms_scale(resid, ffn_gain).astype(jnp.bfloat16)
     experts = lax.axis_size("ep")

time: 116 us -> 97.5 us (0.84)
  waiting for transfers between devices: 36.2 us -> 16.1 us
  blocking collectives: 19.1 us -> 22.4 us
    psum x1 -> x0, waiting for transfers between devices: 20.1 us -> none  [per_device(): lax.psum(partial_value.astype(jnp.bfloat16), 'tp').astype(jnp.float32)]
    all_gather x0 -> x1, blocking collectives: none -> 2.08 us  [per_device(): lax.all_gather(partial_value.astype(jnp.bfloat16), 'tp')]
    all_to_all x1, blocking collectives: 16.9 us -> 18.2 us  [per_device(): lax.all_to_all(outgoing, 'ep', split_axis=0, concat_axis=1, tiled=True)]
  transfers between devices with their start and end apart: 3 -> 2, of which waited for: 3 -> 2; matrix products, arithmetic and copies ran while one was open for 1% -> 0% of each run, Pallas kernels for 0% -> 0%
where the time goes in v1:
time: 97.5 us; the launch traced here: 97 us
  matrix products  27.3 us (28%)
  blocking collectives  22.4 us (23%)
  waiting for transfers between devices  16.1 us (17%)
  between operations  14.4 us (15%)
  other arithmetic  7.05 us (7%)
  starting transfers between devices  6.77 us (7%)
  local copies, waits for them, and re-layouts  2.87 us (3%)
    all_to_all x1, blocking collectives, per_device(): lax.all_to_all(outgoing, 'ep', split_axis=0, concat_axis=1, tiled=True)  18.2 us
    all_to_all x1, waiting for transfers between devices, per_device(): lax.all_to_all(summed, 'ep', split_axis=1, concat_axis=0, tiled=True)  10.2 us
    dot_general x1, matrix products, per_device(): jnp.einsum('shkv,shk->shv', state, key, precision=lax.Precision.HIGHEST)  8.09 us
    dot_general x1, matrix products, per_device(): jnp.einsum('shkv,shk->shv', new_state, query, precision=lax.Precision.HIG...  7.54 us
    all_to_all x1, starting transfers between devices, per_device(): lax.all_to_all(summed, 'ep', split_axis=1, concat_axis=0, tiled=True)  6.73 us
    reduce_scatter x1, waiting for transfers between devices, per_device(): lax.psum_scatter(terms.astype(jnp.bfloat16), 'tp', scatter_dimension=3, t...  5.89 us
    dot_general x6, matrix products, project(): jnp.dot(normed, weight, preferred_element_type=jnp.float32)  5.45 us
    add x1, other arithmetic, per_device(): fade[..., None, None] * state + key[..., :, None] * written[..., None, :]  3.86 us
  transfers between devices with their start and end apart: 2, of which 2 were waited for; matrix products, arithmetic and copies ran while one was open for 0% of the time, Pallas kernels for 0%

profile of v1, /device:TPU:0, one launch (start us, length us, event | category | flops | bytes accessed | tf_op | source)
XLA Modules:
  0.0 97.0 jit_solution(6332632693819059333)
XLA Ops:
  7.2 0.0 reduce-scatter.2.cloned.1.call-start
  7.3 1.2 %fusion.18 = f32[24]{0:T(128)S(1)} fusion(bf16[24,2048]{1,0:T(8,128)(2,1)} %param.19), kind=kLoop, calls=%fused_computation.33 | loop fusion | flops 147432 | bytes 98400 | tf_op jit(solution)/shard_map/reduce_sum | solution.py:10
  8.5 2.1 %fusion.6 = f32[24,512]{1,0:T(8,128)S(1)} fusion(bf16[2048,512]{1,0:T(8,128)(2,1)} %param.22, bf16[24,2048]{1,0:T(8,128)(2,1)} %param.19, f32[2048]{0:T(1024)} %param.20, f32[24]{0:T(128)S(1)} %add_rsqrt_fusion.4), kind=kOutput, calls=%fused_computation.16 | convolution fusion | flops 50552832 | bytes 2252896 | tf_op jit(solution)/shard_map/dot_general | solution.py:46
  10.6 0.1 multiply_reduce_fusion.3
  10.7 0.1 broadcast_multiply_fusion
  10.9 0.2 fusion.34
  11.1 0.1 copy.48
  11.2 2.0 %fusion.5 = f32[24,512]{1,0:T(8,128)S(1)} fusion(bf16[2048,512]{1,0:T(8,128)(2,1)} %param.23, bf16[24,2048]{1,0:T(8,128)(2,1)S(1)} %copy-done.2, f32[2048]{0:T(1024)S(1)} %copy-done.5, f32[24]{0:T(128)S(1)} %add_rsqrt_fusion.4), kind=kOutput, calls=%fused_computation.14 | convolution fusion | flops 50552832 | bytes 2252896 | tf_op jit(solution)/shard_map/dot_general | solution.py:46
  13.3 0.2 fusion.13
  13.5 0.1 copy.49
  13.6 8.1 %fusion.41 = f32[24,4,1,128]{3,2,1,0:T(1,128)S(1)} fusion(f32[24,4,128,1]{2,3,1,0:T(1,128)S(1)} %bitcast.50, f32[24,4,128,128]{3,2,1,0:T(8,128)} %param.29), kind=kOutput, calls=%fused_computation.73 | convolution fusion | flops 18874368 | bytes 6389760 | tf_op jit(solution)/shard_map/shkv,shk->shv/dot_general | solution.py:57
  21.7 0.1 fusion.24
  21.8 3.9 %multiply_add_fusion = f32[24,4,128,128]{3,2,1,0:T(8,128)} fusion(f32[24,4,128,128]{3,2,1,0:T(8,128)S(1)} %copy-done.1, f32[24,4,128]{2,1,0:T(4,128)S(1)} %fusion.24, f32[24,4,128]{2,1,0:T(4,128)S(1)} %broadcast_multiply_fusion, f32[24,4]{1,0:T(8,128)S(1)} %copy.48), kind=kLoop, calls=%fused_computation | loop fusion | flops 4718592 | bytes 12681600 | tf_op jit(solution)/shard_map/add | solution.py:59
  25.7 0.4 fusion.4
  26.2 0.1 multiply_reduce_fusion.2
  26.3 0.1 multiply_multiply_fusion
  26.4 7.5 %fusion.42 = f32[24,4,1,128]{3,2,1,0:T(1,128)S(1)} fusion(f32[24,4,128,128]{3,2,1,0:T(8,128)} %multiply_add_fusion, f32[24,4,128,1]{2,3,1,0:T(1,128)S(1)} %bitcast.53), kind=kOutput, calls=%fused_computation.74 | convolution fusion | flops 18874368 | bytes 6389760 | tf_op jit(solution)/shard_map/shkv,shk->shv/dot_general | solution.py:60
  33.9 0.1 multiply_reduce_fusion.1
  34.1 0.4 fusion.3
  34.5 0.1 copy-done.9
  34.6 0.1 fusion.25
  34.7 0.4 convolution_convert_fusion.1
  35.1 2.1 %all-gather = bf16[48,2048]{1,0:T(8,128)(2,1)S(1)} all-gather(bf16[24,2048]{1,0:T(8,128)(2,1)S(1)} %convolution_convert_fusion.1), channel_id=2, replica_groups=mesh['ep'=16,'tp'=2] {'tp'}, dimensions={0}, use_global_device_ids=true | all-gather | bytes 294912 | tf_op jit(solution)/shard_map/all_gather | solution.py:65
  37.2 0.1 multiply_reduce_fusion
  37.4 0.1 multiply_convert_fusion
  37.5 0.1 broadcast_in_dim.2
  37.6 0.1 copy.51
  37.7 0.1 eq.50
  37.8 0.1 fusion.28
  37.9 0.1 reduce_window_sum.11
  37.9 0.2 select_reduce_fusion
  38.1 0.3 convolution_convert_fusion.2
  38.5 0.1 reshape.136
  38.6 18.2 %all_to_all.21 = bf16[16,1,6,1024]{3,2,1,0:T(8,128)(2,1)S(1)} all-to-all(bf16[16,1,6,1024]{3,2,1,0:T(8,128)(2,1)S(1)} %bitcast.48), channel_id=1, replica_groups=mesh['ep'=16,'tp'=2] {'ep'}, dimensions={0} | all-to-all | bytes 393216 | tf_op jit(solution)/shard_map/all_to_all | solution.py:88
  56.7 2.2 %all-gather.1 = bf16[16,1,6,2048]{3,2,1,0:T(8,128)(2,1)S(1)} all-gather(bf16[16,1,6,1024]{3,2,1,0:T(8,128)(2,1)S(1)} %all_to_all.21), channel_id=3, replica_groups=mesh['ep'=16,'tp'=2] {'tp'}, dimensions={3}, use_global_device_ids=true | all-gather | bytes 589824 | tf_op jit(solution)/shard_map/all_gather | solution.py:87
  58.9 0.1 reshape.137
  59.1 1.5 %fusion.16 = f32[96,256]{1,0:T(8,128)S(1)} fusion(bf16[96,2048]{1,0:T(8,128)(2,1)S(1)} %reshape.137, bf16[1,2048,256]{2,1,0:T(8,128)(2,1)} %param.33), kind=kOutput, calls=%fused_computation.28 | convolution fusion | flops 100663296 | bytes 1540096 | tf_op jit(solution)/shard_map/dot_general | solution.py:94
  60.6 1.5 %fusion.2 = bf16[96,256]{1,0:T(8,128)(2,1)S(1)} fusion(bf16[96,2048]{1,0:T(8,128)(2,1)S(1)} %reshape.137, bf16[1,2048,256]{2,1,0:T(8,128)(2,1)} %param.34, f32[96,256]{1,0:T(8,128)S(1)} %fusion.16), kind=kOutput, calls=%fused_computation.8 | convolution fusion | flops 100810752 | bytes 1589248 | tf_op jit(solution)/shard_map/dot_general | solution.py:95
  62.2 2.3 %fusion = bf16[1,16,6,2048]{3,1,2,0:T(8,128)(2,1)} fusion(bf16[1,256,2048]{2,1,0:T(8,128)(2,1)} %param.35, bf16[16,6,256]{2,1,0:T(8,128)(2,1)S(1)} %dot_general.56), kind=kOutput, calls=%fused_computation.2 | convolution fusion | flops 100859904 | bytes 1490944 | tf_op jit(solution)/shard_map/dot_general | solution.py:97
  64.5 5.9 %reduce-scatter.2.cloned.1.call-done = bf16[1,16,6,1024]{3,1,2,0:T(8,128)(2,1)} async-done(((bf16[1,16,6,2048]{3,1,2,0:T(8,128)(2,1)}), bf16[1,16,6,1024]{3,1,2,0:T(8,128)(2,1)}) %reduce-scatter.2.cloned.1.call-update) | async-done | bytes 196624 | tf_op jit(solution)/shard_map/reduce_scatter | solution.py:99
  70.4 1.7 %copy.55 = bf16[1,16,6,1024]{3,2,0,1:T(8,128)(2,1)} copy(bf16[1,16,6,1024]{3,1,2,0:T(8,128)(2,1)} %reduce-scatter.2.cloned.1.call-done) | data formatting | bytes 393216 | tf_op jit(solution)/shard_map/reduce_scatter | solution.py:99
  72.1 6.7 %all-to-all-start.1 = ((bf16[1,16,6,1024]{3,2,0,1:T(8,128)(2,1)}), bf16[1,16,6,1024]{3,2,0,1:T(8,128)(2,1)S(1)}, u32[]{:S(2)}, u32[]{:S(2)}) async-start(bf16[1,16,6,1024]{3,2,0,1:T(8,128)(2,1)} %copy.55), calls=%async_computation.2 | async-start | bytes 524288 | tf_op jit(solution)/shard_map/all_to_all | solution.py:100
  78.8 0.1 reduce_sum.83
  78.9 0.1 copy.52
  79.0 10.2 %all-to-all-done.1 = bf16[1,16,6,1024]{3,2,0,1:T(8,128)(2,1)S(1)} async-done(((bf16[1,16,6,1024]{3,2,0,1:T(8,128)(2,1)}), bf16[1,16,6,1024]{3,2,0,1:T(8,128)(2,1)S(1)}, u32[]{:S(2)}, u32[]{:S(2)}) %all-to-all-start.1) | async-done | bytes 196640 | tf_op jit(solution)/shard_map/all_to_all | solution.py:100
  89.2 0.1 reshape.151
  89.3 0.2 fusion.1
  89.5 0.6 add_convert_fusion
  (44 shorter events, 0.3 us)
Async XLA Ops:
  7.2 27.5 %copy-start = (bf16[512,2048]{1,0:T(8,128)(2,1)S(1)}, bf16[512,2048]{1,0:T(8,128)(2,1)}, u32[]{:S(2)}) copy-start(bf16[512,2048]{1,0:T(8,128)(2,1)} %param.31) | copy-start | bytes 6291460
  7.2 3.7 %copy-start.2 = (bf16[24,2048]{1,0:T(8,128)(2,1)S(1)}, bf16[24,2048]{1,0:T(8,128)(2,1)}, u32[]{:S(2)}) copy-start(bf16[24,2048]{1,0:T(8,128)(2,1)} %param.19) | copy-start | bytes 294916
  7.2 3.7 %copy-start.5 = (f32[2048]{0:T(1024)S(1)}, f32[2048]{0:T(1024)}, u32[]{:S(2)}) copy-start(f32[2048]{0:T(1024)} %param.20) | copy-start | bytes 24580
  7.2 3.6 %copy-start.12 = (f32[4]{0:T(128)S(1)}, f32[4]{0:T(128)}, u32[]{:S(2)}) copy-start(f32[4]{0:T(128)} %param.27) | copy-start | bytes 52
  7.2 3.7 %copy-start.10 = (bf16[2048,4]{0,1:T(4,128)(2,1)S(1)}, bf16[2048,4]{0,1:T(4,128)(2,1)}, u32[]{:S(2)}) copy-start(bf16[2048,4]{0,1:T(4,128)(2,1)} %param.25) | copy-start | bytes 49156
  7.2 3.7 %copy-start.13 = (f32[4]{0:T(128)S(1)}, f32[4]{0:T(128)}, u32[]{:S(2)}) copy-start(f32[4]{0:T(128)} %param.28) | copy-start | bytes 52
  7.2 63.1 %reduce-scatter.2.cloned.1.call-start = ((), (), s32[]{:S(2)}) async-start(), calls=%async_computation.3 | async-start | bytes 589824 | tf_op jit(solution)/shard_map/reduce_scatter | solution.py:99
  8.4 4.8 %copy-start.11 = (bf16[2048,4]{0,1:T(4,128)(2,1)S(1)}, bf16[2048,4]{0,1:T(4,128)(2,1)}, u32[]{:S(2)}) copy-start(bf16[2048,4]{0,1:T(4,128)(2,1)} %param.26) | copy-start | bytes 49156
  13.6 8.2 %copy-start.1 = (f32[24,4,128,128]{3,2,1,0:T(8,128)S(1)}, f32[24,4,128,128]{3,2,1,0:T(8,128)}, u32[]{:S(2)}) copy-start(f32[24,4,128,128]{3,2,1,0:T(8,128)} %param.29) | copy-start | bytes 18874372
  21.8 3.9 %copy-start.3 = (bf16[2048,512]{1,0:T(8,128)(2,1)S(1)}, bf16[2048,512]{1,0:T(8,128)(2,1)}, u32[]{:S(2)}) copy-start(bf16[2048,512]{1,0:T(8,128)(2,1)} %param.21) | copy-start | bytes 6291460
  26.4 7.7 %copy-start.4 = (bf16[2048,512]{1,0:T(8,128)(2,1)S(1)}, bf16[2048,512]{1,0:T(8,128)(2,1)}, u32[]{:S(2)}) copy-start(bf16[2048,512]{1,0:T(8,128)(2,1)} %param.24) | copy-start | bytes 6291460
  33.9 0.7 copy-start.9
  34.5 2.9 %copy-start.7 = (f32[2048]{0:T(1024)S(1)}, f32[2048]{0:T(1024)}, u32[]{:S(2)}) copy-start(f32[2048]{0:T(1024)} %param.32) | copy-start | bytes 24580
  34.5 3.1 %copy-start.6 = (s32[24,2]{0,1:T(2,128)S(1)}, s32[24,2]{0,1:T(2,128)}, u32[]{:S(2)}) copy-start(s32[24,2]{0,1:T(2,128)} %param.36) | copy-start | bytes 580
  62.1 27.2 %copy-start.8 = (f32[24,2]{0,1:T(2,128)S(1)}, f32[24,2]{0,1:T(2,128)}, u32[]{:S(2)}) copy-start(f32[24,2]{0,1:T(2,128)} %param.37) | copy-start | bytes 580
  72.1 17.1 %all-to-all-start.1 = ((bf16[1,16,6,1024]{3,2,0,1:T(8,128)(2,1)}), bf16[1,16,6,1024]{3,2,0,1:T(8,128)(2,1)S(1)}, u32[]{:S(2)}, u32[]{:S(2)}) async-start(bf16[1,16,6,1024]{3,2,0,1:T(8,128)(2,1)} %copy.55), calls=%async_computation.2 | async-start | bytes 524288 | tf_op jit(solution)/shard_map/all_to_all | solution.py:100
Sparse Core Ops, SparseCore 0:
  64.6 5.7 reduce-scatter.1
